TPU v7x, 32 devices: a whole 2x2x4 slice. The times are simulated.
32 devices in a mesh: dp: 2 (over x), kv: 8 (over z, y), tp: 2 (over core).
Axes of the slice: x: 2, y: 2, z: 4, core: 2. Of those that a mesh axis runs over, the one named last changes fastest.
Arguments:
- tokens: bfloat16 [48, 2048], P('dp', ('kv', 'tp')), may hold values from -21 to 21
- state: float32 [48, 8, 128, 128], P(('dp', 'kv'), 'tp'), may hold values from -3 to 3
- mix_gain: bfloat16 [2048], P(('kv', 'tp')), may hold values from 0.099609375 to 1.8984375
- w_query: bfloat16 [2048, 1024], P('kv', 'tp'), may hold values from -0.125 to 0.125
- w_key: bfloat16 [2048, 1024], P('kv', 'tp'), may hold values from -0.125 to 0.125
- w_value: bfloat16 [2048, 1024], P('kv', 'tp'), may hold values from -0.125 to 0.125
- w_beta: bfloat16 [2048, 8], P('kv', 'tp'), may hold values from -0.125 to 0.125
- w_decay: bfloat16 [2048, 8], P('kv', 'tp'), may hold values from -0.125 to 0.125
- decay_log: float32 [8], P('tp'), may hold values from -1.5 to 1
- head_gain: bfloat16 [128], replicated, may hold values from 0.099609375 to 1.8984375
- w_out: bfloat16 [1024, 2048], P('tp', 'kv'), may hold values from -0.1875 to 0.1875
- ff_gain: bfloat16 [2048], P(('kv', 'tp')), may hold values from 0.099609375 to 1.8984375
- w_up: bfloat16 [2048, 8192], P(None, ('kv', 'tp')), may hold values from -0.125 to 0.125
- w_down: bfloat16 [8192, 2048], P(('kv', 'tp')), may hold values from -0.09375 to 0.09375
Outputs:
- output: bfloat16 [48, 2048], P('dp', ('kv', 'tp'))
- new_state: float32 [48, 8, 128, 128], P(('dp', 'kv'), 'tp')
All inputs are finite; a program needn't handle non-finite values.
Results may differ from a plain program's by a relative error of at most 0.013.
Values may be sent and summed in bfloat16 or wider, within the bound.
No kernel may reach another device: no remote copies, remote signals or barrier semaphores. Data moves between devices by JAX's collectives and lax.ppermute only.
A program may use at most 64 MiB of HBM per device.

v0:
```python
import functools
import jax
import jax.numpy as jnp
from jax import lax
from jax.sharding import PartitionSpec as P

BF = jnp.bfloat16
F32 = jnp.float32


def split_pair(value):
    high = value.astype(BF)
    low = (value - lax.reduce_precision(value, 8, 7)).astype(BF)
    return (high, low)


def local(
    tokens,
    state,
    mix_gain,
    w_query,
    w_key,
    w_value,
    w_beta,
    w_decay,
    decay_log,
    head_gain,
    w_out,
    ff_gain,
    w_up,
    w_down,
    n_kv,
    n_tp,
):
    rows, width = tokens.shape
    seq, heads, size = state.shape[:3]
    n_all = n_kv * n_tp
    model = width * n_all
    keys = heads * size
    packed = jnp.concatenate([tokens, mix_gain[None, :]], axis=0)
    wide = lax.all_gather(packed, "tp", axis=1, tiled=True)
    tp_at = lax.axis_index("tp")
    out_cols = []
    for step in range(n_tp):
        target = (tp_at + step) % n_tp
        block = lax.dynamic_slice_in_dim(w_out, target * width, width, axis=1)
        if step:
            block = lax.ppermute(block, "tp", [(i, (i + step) % n_tp) for i in range(n_tp)])
        out_cols.append(block)
    wide_float = wide[:rows].astype(F32)
    scaled = (wide_float * wide[rows:].astype(F32)).astype(BF)
    dot = functools.partial(jnp.dot, preferred_element_type=F32)
    gates_part = dot(scaled, jnp.concatenate([w_beta, w_decay], axis=1))
    square_part = jnp.sum(wide_float * wide_float, axis=1, keepdims=True)
    small = jnp.concatenate([gates_part, square_part], axis=1)
    high, low = split_pair(small)
    n_small = small.shape[1]
    pad = jnp.zeros((rows, size - 2 * n_small), BF)
    sent = jnp.concatenate(
        [
            dot(scaled, w_query).astype(BF),
            dot(scaled, w_key).astype(BF),
            dot(scaled, w_value).astype(BF),
            high,
            low,
            pad,
        ],
        axis=1,
    ).reshape(n_kv, seq, 3 * keys + size)
    got = lax.all_to_all(sent, "kv", 0, 0, tiled=False)
    total = jnp.sum(got.astype(F32), axis=0)
    small = (
        total[:, 3 * keys : 3 * keys + n_small]
        + total[:, 3 * keys + n_small : 3 * keys + 2 * n_small]
    )
    inverse = lax.rsqrt(small[:, 2 * heads :] / model + 1e-06)
    query = (inverse * total[:, :keys]).reshape(seq, heads, size)
    key_rows = (inverse * total[:, keys : 2 * keys]).reshape(seq, heads, size)
    value = (inverse * total[:, 2 * keys : 3 * keys]).reshape(seq, heads, size)
    beta = jax.nn.sigmoid(inverse * small[:, :heads])
    decay = -jnp.exp(decay_log)[None, :] * jax.nn.softplus(inverse * small[:, heads : 2 * heads])
    qnorm = query * lax.rsqrt(jnp.sum(query * query, axis=-1, keepdims=True) + 1e-06)
    knorm = key_rows * lax.rsqrt(jnp.sum(key_rows * key_rows, axis=-1, keepdims=True) + 1e-06)
    kept = state * jnp.exp(decay)[:, :, None, None]
    predicted = jnp.sum(kept * knorm[:, :, :, None], axis=2)
    new_state = (
        kept + (beta[:, :, None] * knorm)[:, :, :, None] * (value - predicted)[:, :, None, :]
    )
    read = jnp.sum(new_state * qnorm[:, :, :, None], axis=2) / jnp.sqrt(jnp.float32(size))
    normed = (
        read
        * lax.rsqrt(jnp.mean(read * read, axis=-1, keepdims=True) + 1e-06)
        * head_gain.astype(F32)
    )
    normed = normed.astype(BF).reshape(seq, keys)
    axes = ("kv", "tp")
    spread = lax.all_to_all(
        jnp.broadcast_to(normed[None], (n_all, seq, keys)), axes, 0, 0, tiled=False
    )
    spread = spread.reshape(n_kv, n_tp, seq, keys)
    mixed = 0.0
    for step in range(n_tp):
        heads_of = lax.dynamic_index_in_dim(spread, (tp_at - step) % n_tp, 1, keepdims=False)
        part = dot(heads_of.reshape(rows, keys), out_cols[step])
        mixed = mixed + lax.reduce_precision(part, 8, 7)
    resid = (tokens.astype(F32) + mixed).astype(BF)
    resid_float = resid.astype(F32)
    scaled2 = (resid_float * ff_gain.astype(F32)[None, :]).astype(BF)
    high, low = split_pair(jnp.sum(resid_float * resid_float, axis=1))
    tail_rows = -(-2 * rows // width // 8) * 8
    tail = jnp.concatenate([high, low, jnp.zeros((tail_rows * width - 2 * rows,), BF)])
    tail = tail.reshape(tail_rows, width)
    sent2 = jnp.concatenate([scaled2, tail], axis=0)
    got2 = lax.all_to_all(
        jnp.broadcast_to(sent2[None], (n_all,) + sent2.shape), axes, 0, 0, tiled=False
    )
    sums = jnp.sum(
        got2[:, rows:].reshape(n_all, tail_rows * width)[:, : 2 * rows].astype(F32), axis=0
    )
    inverse2 = lax.rsqrt((sums[:rows] + sums[rows:]) / model + 1e-06)[:, None]
    whole = got2[:, :rows].transpose(1, 0, 2).reshape(rows, model)
    up_rows = dot(whole, w_up) * inverse2
    act = jnp.square(jax.nn.relu(up_rows)).astype(BF)
    down = dot(act, w_down).astype(BF).reshape(rows, n_all, width).transpose(1, 0, 2)
    got3 = lax.all_to_all(down, axes, 0, 0, tiled=False)
    output = (resid_float + jnp.sum(got3.astype(F32), axis=0)).astype(BF)
    return (output, new_state)


def solution(mesh):
    placed = (
        P("dp", ("kv", "tp")),
        P(("dp", "kv"), "tp", None, None),
        P(("kv", "tp")),
        P("kv", "tp"),
        P("kv", "tp"),
        P("kv", "tp"),
        P("kv", "tp"),
        P("kv", "tp"),
        P("tp"),
        P(),
        P("tp", "kv"),
        P(("kv", "tp")),
        P(None, ("kv", "tp")),
        P(("kv", "tp"), None),
    )
    return jax.shard_map(
        functools.partial(local, n_kv=mesh.shape["kv"], n_tp=mesh.shape["tp"]),
        mesh=mesh,
        in_specs=placed,
        out_specs=(P("dp", ("kv", "tp")), P(("dp", "kv"), "tp", None, None)),
        check_vma=False,
    )
```

profile of v0, /device:TPU:0, one launch (start us, length us, event | category | flops | bytes accessed | tf_op | source)
XLA Modules:
  0.0 61.9 jit_solution(8024021234024849064)
XLA Ops:
  0.7 0.9 %pad_maximum_fusion.1 = bf16[25,128]{1,0:T(8,128)(2,1)S(1)} fusion(bf16[1,128]{1,0:T(2,128)(2,1)} %bitcast.53, bf16[24,128]{1,0:T(8,128)(2,1)} %param.14), kind=kLoop, calls=%fused_computation.43 | loop fusion | flops 12800 | bytes 12800 | tf_op jit(solution)/shard_map/concatenate | solution.py:40
  1.5 2.1 %all_gather.3 = bf16[25,256]{1,0:T(8,128)(2,1)S(1)} all-gather(bf16[25,128]{1,0:T(8,128)(2,1)S(1)} %pad_maximum_fusion.1), channel_id=1, replica_groups=mesh['dp'=2,'kv'=8,'tp'=2] {'tp'}, dimensions={1}, use_global_device_ids=true | all-gather | bytes 19200 | tf_op jit(solution)/shard_map/all_gather | solution.py:41
  3.6 0.1 fusion.14
  3.8 0.8 %fusion.19 = f32[24,8]{1,0:T(8,128)S(1)} fusion(bf16[256,4]{0,1:T(4,128)(2,1)} %param.21, bf16[256,4]{0,1:T(4,128)(2,1)} %param.20, f32[256]{0:T(256)S(1)} %bitcast.48, bf16[25,256]{1,0:T(8,128)(2,1)S(1)} %all_gather.3), kind=kOutput, calls=%fused_computation.51 | convolution fusion | flops 124928 | bytes 18176 | tf_op jit(solution)/shard_map/dot_general | solution.py:53
  4.8 1.1 %convolution_convert_fusion.2 = bf16[24,512]{1,0:T(8,128)(2,1)S(1)} fusion(bf16[256,512]{1,0:T(8,128)(2,1)} %param.18, f32[256]{0:T(256)S(1)} %bitcast.49, bf16[25,256]{1,0:T(8,128)(2,1)S(1)} %all_gather.3), kind=kOutput, calls=%fused_computation.6 | convolution fusion | flops 6322176 | bytes 300032 | tf_op jit(solution)/shard_map/dot_general | solution.py:62
  5.9 1.1 %convolution_convert_fusion.1 = bf16[24,512]{1,0:T(8,128)(2,1)S(1)} fusion(bf16[256,512]{1,0:T(8,128)(2,1)} %param.19, f32[256]{0:T(256)S(1)} %bitcast.50, bf16[25,256]{1,0:T(8,128)(2,1)S(1)} %all_gather.3), kind=kOutput, calls=%fused_computation.5 | convolution fusion | flops 6322176 | bytes 300032 | tf_op jit(solution)/shard_map/dot_general | solution.py:63
  7.1 1.1 %convolution_convert_fusion.3 = bf16[24,512]{1,0:T(8,128)(2,1)S(1)} fusion(bf16[256,512]{1,0:T(8,128)(2,1)} %param.17, f32[256]{0:T(256)S(1)} %bitcast.51, bf16[25,256]{1,0:T(8,128)(2,1)S(1)} %all_gather.3), kind=kOutput, calls=%fused_computation.7 | convolution fusion | flops 6322176 | bytes 300032 | tf_op jit(solution)/shard_map/dot_general | solution.py:61
  8.2 0.1 concatenate.21
  8.3 0.7 %reshape.114 = bf16[8,3,1664]{2,1,0:T(4,128)(2,1)} reshape(bf16[24,1664]{1,0:T(8,128)(2,1)S(1)} %concatenate.21) | data formatting | bytes 159744 | tf_op jit(solution)/shard_map/reshape | solution.py:69
  9.0 7.2 %all-to-all-start = ((bf16[8,3,1664]{2,1,0:T(4,128)(2,1)}), bf16[8,3,1664]{2,1,0:T(4,128)(2,1)S(1)}, u32[]{:S(2)}, u32[]{:S(2)}) async-start(bf16[8,3,1664]{2,1,0:T(4,128)(2,1)} %reshape.114), calls=%async_computation | async-start | bytes 212992 | tf_op jit(solution)/shard_map/all_to_all | solution.py:70
  16.2 0.7 %convert_element_type.80 = f32[128]{0:T(128)S(1)} convert(bf16[128]{0:T(256)(128)(2,1)} %param.23) | non-fusion elementwise | flops 128 | bytes 768 | tf_op jit(solution)/shard_map/convert_element_type | solution.py:93
  16.8 0.7 %exponential_negate_fusion = f32[4]{0:T(128)S(1)} fusion(f32[4]{0:T(128)} %param.22), kind=kLoop, calls=%fused_computation.77 | loop fusion | flops 4 | bytes 32 | tf_op jit(solution)/shard_map/neg | solution.py:81
  17.5 5.9 %all-to-all-done = bf16[8,3,1664]{2,1,0:T(4,128)(2,1)S(1)} async-done(((bf16[8,3,1664]{2,1,0:T(4,128)(2,1)}), bf16[8,3,1664]{2,1,0:T(4,128)(2,1)S(1)}, u32[]{:S(2)}, u32[]{:S(2)}) %all-to-all-start) | async-done | bytes 79904 | tf_op jit(solution)/shard_map/all_to_all | solution.py:70
  23.5 0.2 rsqrt_reduce_fusion
  24.0 0.1 copy.98
  24.1 0.1 copy.86
  24.3 0.1 copy.99
  24.4 0.1 copy.88
  24.6 0.3 multiply_reduce_fusion.1
  24.9 1.4 %multiply_reduce_fusion = (f32[3,4,128]{2,1,0:T(4,128)S(1)}, f32[3,4,128,128]{3,2,1,0:T(8,128)}) fusion(f32[3,4,128]{2,1,0:T(4,128)S(1)} %get-tuple-element.18, f32[3,4,128]{2,1,0:T(4,128)S(1)} %sub.17, f32[3,4,128]{2,1,0:T(4,128)S(1)} %get-tuple-element.4, f32[3,4,128,128]{3,2,1,0:T(8,128)S(1)} %copy-done.1, f32[3,4]{1,0:T(4,128)S(1)} %get-tuple-element.13), kind=kLoop, calls=%fused_computation.15 | loop fusion | flops 981504 | bytes 1597488 | tf_op jit(solution)/shard_map/reduce_sum | solution.py:89
  26.3 0.1 copy.89
  26.4 0.1 copy.90
  26.6 0.6 %broadcast_in_dim.15 = bf16[16,3,512]{2,1,0:T(4,128)(2,1)} broadcast(bf16[3,512]{1,0:T(4,128)(2,1)S(1)} %fusion.18), dimensions={1,2} | broadcast | bytes 52224 | tf_op jit(solution)/shard_map/broadcast_in_dim | solution.py:98
  27.3 3.5 %all-to-all-start.1 = ((bf16[16,3,512]{2,1,0:T(4,128)(2,1)}), bf16[16,3,512]{2,1,0:T(4,128)(2,1)S(1)}, u32[]{:S(2)}, u32[]{:S(2)}) async-start(bf16[16,3,512]{2,1,0:T(4,128)(2,1)} %broadcast_in_dim.15), calls=%async_computation.1 | async-start | bytes 131072 | tf_op jit(solution)/shard_map/all_to_all | solution.py:97
  30.8 0.4 collective-permute-start
  31.2 6.5 %all-to-all-done.1 = bf16[16,3,512]{2,1,0:T(4,128)(2,1)S(1)} async-done(((bf16[16,3,512]{2,1,0:T(4,128)(2,1)}), bf16[16,3,512]{2,1,0:T(4,128)(2,1)S(1)}, u32[]{:S(2)}, u32[]{:S(2)}) %all-to-all-start.1) | async-done | bytes 49184 | tf_op jit(solution)/shard_map/all_to_all | solution.py:97
  37.7 0.1 convolution_reduce-precision_fusion.1
  37.9 0.2 multiply_convert_fusion
  38.3 10.5 %all_to_all.20 = bf16[16,32,128]{2,1,0:T(8,128)(2,1)S(1)} all-to-all(bf16[16,32,128]{2,1,0:T(8,128)(2,1)S(1)} %broadcast_in_dim.17), channel_id=1, replica_groups=mesh['dp'=2,'kv'=8,'tp'=2] {'kv','tp'}, dimensions={0} | all-to-all | bytes 262144 | tf_op jit(solution)/shard_map/all_to_all | solution.py:114
  48.9 2.3 %fusion = bf16[3,16,8,128]{3,2,1,0:T(8,128)(2,1)S(1)} fusion(bf16[512,2048]{1,0:T(8,128)(2,1)S(1)} %copy-done, bf16[2048,512]{1,0:T(8,128)(2,1)} %param.26, f32[24]{0:T(128)S(1)} %add_rsqrt_fusion.2, bf16[16,32,128]{2,1,0:T(8,128)(2,1)S(1)} %all_to_all.20), kind=kOutput, calls=%fused_computation.1 | convolution fusion | flops 100761600 | bytes 4391424 | tf_op jit(solution)/shard_map/dot_general | solution.py:124
  51.3 10.0 %all_to_all.21 = bf16[16,24,128]{2,1,0:T(8,128)(2,1)S(1)} all-to-all(bf16[16,24,128]{2,1,0:T(8,128)(2,1)S(1)} %bitcast.44), channel_id=1, replica_groups=mesh['dp'=2,'kv'=8,'tp'=2] {'kv','tp'}, dimensions={0} | all-to-all | bytes 196608 | tf_op jit(solution)/shard_map/all_to_all | solution.py:125
  61.3 0.6 add_convert_fusion
  (50 shorter events, 1.5 us)
Async XLA Ops:
  0.6 48.3 %copy-start = (bf16[512,2048]{1,0:T(8,128)(2,1)S(1)}, bf16[512,2048]{1,0:T(8,128)(2,1)}, u32[]{:S(2)}) copy-start(bf16[512,2048]{1,0:T(8,128)(2,1)} %param.27) | copy-start | bytes 6291460
  0.6 23.9 %copy-start.1 = (f32[3,4,128,128]{3,2,1,0:T(8,128)S(1)}, f32[3,4,128,128]{3,2,1,0:T(8,128)}, u32[]{:S(2)}) copy-start(f32[3,4,128,128]{3,2,1,0:T(8,128)} %param.15) | copy-start | bytes 2359300
  5.9 24.9 %copy-start.2 = (bf16[512,256]{1,0:T(8,128)(2,1)S(1)}, bf16[512,256]{1,0:T(8,128)(2,1)}, u32[]{:S(2)}) copy-start(bf16[512,256]{1,0:T(8,128)(2,1)} %param.24) | copy-start | bytes 786436
  7.1 24.1 %copy-start.4 = (bf16[128]{0:T(256)(128)(2,1)S(1)}, bf16[128]{0:T(256)(128)(2,1)}, u32[]{:S(2)}) copy-start(bf16[128]{0:T(256)(128)(2,1)} %param.25) | copy-start | bytes 772
  8.3 29.6 %copy-start.3 = (bf16[24,128]{1,0:T(8,128)(2,1)S(1)}, bf16[24,128]{1,0:T(8,128)(2,1)}, u32[]{:S(2)}) copy-start(bf16[24,128]{1,0:T(8,128)(2,1)} %param.14) | copy-start | bytes 18436
  9.0 14.3 %all-to-all-start = ((bf16[8,3,1664]{2,1,0:T(4,128)(2,1)}), bf16[8,3,1664]{2,1,0:T(4,128)(2,1)S(1)}, u32[]{:S(2)}, u32[]{:S(2)}) async-start(bf16[8,3,1664]{2,1,0:T(4,128)(2,1)} %reshape.114), calls=%async_computation | async-start | bytes 212992 | tf_op jit(solution)/shard_map/all_to_all | solution.py:70
  27.3 10.4 %all-to-all-start.1 = ((bf16[16,3,512]{2,1,0:T(4,128)(2,1)}), bf16[16,3,512]{2,1,0:T(4,128)(2,1)S(1)}, u32[]{:S(2)}, u32[]{:S(2)}) async-start(bf16[16,3,512]{2,1,0:T(4,128)(2,1)} %broadcast_in_dim.15), calls=%async_computation.1 | async-start | bytes 131072 | tf_op jit(solution)/shard_map/all_to_all | solution.py:97
  30.8 7.1 %collective-permute-start = (bf16[512,128]{1,0:T(8,128)(2,1)S(1)}, bf16[512,128]{1,0:T(8,128)(2,1)S(1)}, u32[]{:S(2)}, u32[]{:S(2)}) collective-permute-start(bf16[512,128]{1,0:T(8,128)(2,1)S(1)} %constant_dynamic-slice_fusion), channel_id=1, source_target_pairs={{0,1},{1,0},{2,3},{3,2},{4,5},{5,4},{6,7},{7,6},{8,9},{9,8},{10,11... | collective-permute-start | bytes 393224 | tf_op jit(solution)/shard_map/ppermute | solution.py:48
where the time goes:
time: 62.4 us; the launch traced here: 61.9 us
  blocking collectives  22.6 us (36%)
  waiting for transfers between devices  12.3 us (20%)
  starting transfers between devices  11 us (18%)
  matrix products  6.93 us (11%)
  other arithmetic  5.89 us (9%)
  local copies, waits for them, and re-layouts  2.36 us (4%)
  between operations  0.78 us (1%)
    all_to_all x1, blocking collectives, local(): lax.all_to_all(jnp.broadcast_to(sent2[None], (n_all,) + sent2.shape), axe...  10.5 us
    all_to_all x1, blocking collectives, local(): got3 = lax.all_to_all(down, axes, 0, 0, tiled=False)  9.96 us
    all_to_all x1, starting transfers between devices, local(): got = lax.all_to_all(sent, 'kv', 0, 0, tiled=False)  7.16 us
    all_to_all x1, waiting for transfers between devices, local(): lax.all_to_all(jnp.broadcast_to(normed[None], (n_all, seq, keys)), axes,...  6.46 us
    all_to_all x1, waiting for transfers between devices, local(): got = lax.all_to_all(sent, 'kv', 0, 0, tiled=False)  5.86 us
    all_to_all x1, starting transfers between devices, local(): lax.all_to_all(jnp.broadcast_to(normed[None], (n_all, seq, keys)), axes,...  3.5 us
    dot_general x1, matrix products, local(): dot(act, w_down).astype(BF).reshape(rows, n_all, width).transpose(1, 0, 2)  2.35 us
    all_gather x1, blocking collectives, local(): wide = lax.all_gather(packed, 'tp', axis=1, tiled=True)  2.11 us
  transfers between devices with their start and end apart: 3, of which 2 were waited for; matrix products, arithmetic and copies ran while one was open for 3% of the time, Pallas kernels for 0%

commit v1 on v0

--- a/solution.py
+++ b/solution.py
@@ -38,7 +38,9 @@
     model = width * n_all
     keys = heads * size
     packed = jnp.concatenate([tokens, mix_gain[None, :]], axis=0)
-    wide = lax.all_gather(packed, "tp", axis=1, tiled=True)
+    wide = jnp.concatenate(
+        lax.all_to_all(jnp.stack([packed] * lax.axis_size("tp")), "tp", 0, 0), axis=1
+    )
     tp_at = lax.axis_index("tp")
     out_cols = []
     for step in range(n_tp):

time: 62.4 us -> 64.2 us (1.029)
  blocking collectives: 22.6 us -> 24.2 us
    all_to_all x0 -> x1, blocking collectives: none -> 3.72 us  [local(): lax.all_to_all(jnp.stack([packed] * lax.axis_size('tp')), 'tp', 0, 0)]
    all_gather x1 -> x0, blocking collectives: 2.11 us -> none  [local(): wide = lax.all_gather(packed, 'tp', axis=1, tiled=True)]
    another operation x0 -> x2, other arithmetic: none -> 0.88 us  [local(): jnp.stack([packed] * lax.axis_size('tp'))]
    concatenate x1 -> x0, other arithmetic: 0.87 us -> none  [local(): packed = jnp.concatenate([tokens, mix_gain[None, :]], axis=0)]
  transfers between devices with their start and end apart: 3 -> 3, of which waited for: 2 -> 2; matrix products, arithmetic and copies ran while one was open for 3% -> 2% of each run, Pallas kernels for 0% -> 0%
where the time goes in v1:
time: 64.2 us; the launch traced here: 63.6 us
  blocking collectives  24.2 us (38%)
  waiting for transfers between devices  12.3 us (19%)
  starting transfers between devices  11.2 us (17%)
  matrix products  6.93 us (11%)
  other arithmetic  5.89 us (9%)
  local copies, waits for them, and re-layouts  2.36 us (4%)
  between operations  0.78 us (1%)
    all_to_all x1, blocking collectives, local(): lax.all_to_all(jnp.broadcast_to(sent2[None], (n_all,) + sent2.shape), axe...  10.5 us
    all_to_all x1, blocking collectives, local(): got3 = lax.all_to_all(down, axes, 0, 0, tiled=False)  9.96 us
    all_to_all x1, starting transfers between devices, local(): got = lax.all_to_all(sent, 'kv', 0, 0, tiled=False)  7.31 us
    all_to_all x1, waiting for transfers between devices, local(): lax.all_to_all(jnp.broadcast_to(normed[None], (n_all, seq, keys)), axes,...  6.46 us
    all_to_all x1, waiting for transfers between devices, local(): got = lax.all_to_all(sent, 'kv', 0, 0, tiled=False)  5.86 us
    all_to_all x1, blocking collectives, local(): lax.all_to_all(jnp.stack([packed] * lax.axis_size('tp')), 'tp', 0, 0)  3.72 us
    all_to_all x1, starting transfers between devices, local(): lax.all_to_all(jnp.broadcast_to(normed[None], (n_all, seq, keys)), axes,...  3.5 us
    dot_general x1, matrix products, local(): dot(act, w_down).astype(BF).reshape(rows, n_all, width).transpose(1, 0, 2)  2.35 us
  transfers between devices with their start and end apart: 3, of which 2 were waited for; matrix products, arithmetic and copies ran while one was open for 2% of the time, Pallas kernels for 0%

profile of v1, /device:TPU:0, one launch (start us, length us, event | category | flops | bytes accessed | tf_op | source)
XLA Modules:
  0.0 63.6 jit_solution(3839806584038207954)
XLA Ops:
  0.7 0.9 %maximum_bitcast_fusion = bf16[1,25,128]{2,1,0:T(8,128)(2,1)S(1)} fusion(bf16[1,128]{1,0:T(2,128)(2,1)} %bitcast.97, bf16[24,128]{1,0:T(8,128)(2,1)} %param.14), kind=kLoop, calls=%fused_computation.45 | loop fusion | flops 12800 | bytes 12800 | tf_op jit(solution)/shard_map/stack | solution.py:42
  1.5 3.7 %all_to_all.25 = bf16[2,25,128]{2,1,0:T(8,128)(2,1)S(1)} all-to-all(bf16[2,25,128]{2,1,0:T(8,128)(2,1)S(1)} %pad_maximum_fusion), channel_id=1, replica_groups=mesh['dp'=2,'kv'=8,'tp'=2] {'tp'}, dimensions={0} | all-to-all | bytes 25600 | tf_op jit(solution)/shard_map/all_to_all | solution.py:42
  5.3 0.1 fusion.13
  5.5 0.8 %fusion.19 = f32[24,8]{1,0:T(8,128)S(1)} fusion(bf16[256,4]{0,1:T(4,128)(2,1)} %param.21, bf16[256,4]{0,1:T(4,128)(2,1)} %param.20, f32[256]{0:T(256)S(1)} %bitcast.92, bf16[25,2,128]{2,0,1:T(8,128)(2,1)S(1)} %bitcast.85), kind=kOutput, calls=%fused_computation.53 | convolution fusion | flops 124928 | bytes 18176 | tf_op jit(solution)/shard_map/dot_general | solution.py:55
  6.5 1.1 %convolution_convert_fusion.2 = bf16[24,512]{1,0:T(8,128)(2,1)S(1)} fusion(bf16[256,512]{1,0:T(8,128)(2,1)} %param.18, f32[256]{0:T(256)S(1)} %bitcast.93, bf16[25,2,128]{2,0,1:T(8,128)(2,1)S(1)} %bitcast.86), kind=kOutput, calls=%fused_computation.6 | convolution fusion | flops 6322176 | bytes 300032 | tf_op jit(solution)/shard_map/dot_general | solution.py:64
  7.5 1.1 %convolution_convert_fusion.1 = bf16[24,512]{1,0:T(8,128)(2,1)S(1)} fusion(bf16[256,512]{1,0:T(8,128)(2,1)} %param.19, f32[256]{0:T(256)S(1)} %bitcast.94, bf16[25,2,128]{2,0,1:T(8,128)(2,1)S(1)} %bitcast.87), kind=kOutput, calls=%fused_computation.5 | convolution fusion | flops 6322176 | bytes 300032 | tf_op jit(solution)/shard_map/dot_general | solution.py:65
  8.7 1.1 %convolution_convert_fusion.3 = bf16[24,512]{1,0:T(8,128)(2,1)S(1)} fusion(bf16[256,512]{1,0:T(8,128)(2,1)} %param.17, f32[256]{0:T(256)S(1)} %bitcast.95, bf16[25,2,128]{2,0,1:T(8,128)(2,1)S(1)} %bitcast.88), kind=kOutput, calls=%fused_computation.7 | convolution fusion | flops 6322176 | bytes 300032 | tf_op jit(solution)/shard_map/dot_general | solution.py:63
  9.8 0.1 concatenate.21
  9.9 0.7 %reshape.132 = bf16[8,3,1664]{2,1,0:T(4,128)(2,1)} reshape(bf16[24,1664]{1,0:T(8,128)(2,1)S(1)} %concatenate.21) | data formatting | bytes 159744 | tf_op jit(solution)/shard_map/reshape | solution.py:71
  10.6 7.3 %all-to-all-start.1 = ((bf16[8,3,1664]{2,1,0:T(4,128)(2,1)}), bf16[8,3,1664]{2,1,0:T(4,128)(2,1)S(1)}, u32[]{:S(2)}, u32[]{:S(2)}) async-start(bf16[8,3,1664]{2,1,0:T(4,128)(2,1)} %reshape.132), calls=%async_computation.1 | async-start | bytes 212992 | tf_op jit(solution)/shard_map/all_to_all | solution.py:72
  17.9 0.7 %convert_element_type.100 = f32[128]{0:T(128)S(1)} convert(bf16[128]{0:T(256)(128)(2,1)} %param.23) | non-fusion elementwise | flops 128 | bytes 768 | tf_op jit(solution)/shard_map/convert_element_type | solution.py:95
  18.6 0.7 %exponential_negate_fusion = f32[4]{0:T(128)S(1)} fusion(f32[4]{0:T(128)} %param.22), kind=kLoop, calls=%fused_computation.79 | loop fusion | flops 4 | bytes 32 | tf_op jit(solution)/shard_map/neg | solution.py:83
  19.3 5.9 %all-to-all-done.1 = bf16[8,3,1664]{2,1,0:T(4,128)(2,1)S(1)} async-done(((bf16[8,3,1664]{2,1,0:T(4,128)(2,1)}), bf16[8,3,1664]{2,1,0:T(4,128)(2,1)S(1)}, u32[]{:S(2)}, u32[]{:S(2)}) %all-to-all-start.1) | async-done | bytes 79904 | tf_op jit(solution)/shard_map/all_to_all | solution.py:72
  25.2 0.2 rsqrt_reduce_fusion
  25.7 0.1 copy.104
  25.8 0.1 copy.92
  26.0 0.1 copy.105
  26.1 0.1 copy.94
  26.3 0.3 multiply_reduce_fusion.1
  26.7 1.4 %multiply_reduce_fusion = (f32[3,4,128]{2,1,0:T(4,128)S(1)}, f32[3,4,128,128]{3,2,1,0:T(8,128)}) fusion(f32[3,4,128]{2,1,0:T(4,128)S(1)} %get-tuple-element.18, f32[3,4,128]{2,1,0:T(4,128)S(1)} %sub.17, f32[3,4,128]{2,1,0:T(4,128)S(1)} %get-tuple-element.4, f32[3,4,128,128]{3,2,1,0:T(8,128)S(1)} %copy-done.1, f32[3,4]{1,0:T(4,128)S(1)} %get-tuple-element.13), kind=kLoop, calls=%fused_computation.15 | loop fusion | flops 981504 | bytes 1597488 | tf_op jit(solution)/shard_map/reduce_sum | solution.py:91
  28.1 0.1 copy.95
  28.2 0.1 copy.96
  28.4 0.6 %broadcast_in_dim.15 = bf16[16,3,512]{2,1,0:T(4,128)(2,1)} broadcast(bf16[3,512]{1,0:T(4,128)(2,1)S(1)} %fusion.18), dimensions={1,2} | broadcast | bytes 52224 | tf_op jit(solution)/shard_map/broadcast_in_dim | solution.py:100
  29.0 3.5 %all-to-all-start.2 = ((bf16[16,3,512]{2,1,0:T(4,128)(2,1)}), bf16[16,3,512]{2,1,0:T(4,128)(2,1)S(1)}, u32[]{:S(2)}, u32[]{:S(2)}) async-start(bf16[16,3,512]{2,1,0:T(4,128)(2,1)} %broadcast_in_dim.15), calls=%async_computation.2 | async-start | bytes 131072 | tf_op jit(solution)/shard_map/all_to_all | solution.py:99
  32.6 0.4 collective-permute-start
  32.9 6.5 %all-to-all-done.2 = bf16[16,3,512]{2,1,0:T(4,128)(2,1)S(1)} async-done(((bf16[16,3,512]{2,1,0:T(4,128)(2,1)}), bf16[16,3,512]{2,1,0:T(4,128)(2,1)S(1)}, u32[]{:S(2)}, u32[]{:S(2)}) %all-to-all-start.2) | async-done | bytes 49184 | tf_op jit(solution)/shard_map/all_to_all | solution.py:99
  39.5 0.1 convolution_reduce-precision_fusion.1
  39.7 0.2 multiply_convert_fusion
  40.0 10.5 %all_to_all.26 = bf16[16,32,128]{2,1,0:T(8,128)(2,1)S(1)} all-to-all(bf16[16,32,128]{2,1,0:T(8,128)(2,1)S(1)} %broadcast_in_dim.17), channel_id=1, replica_groups=mesh['dp'=2,'kv'=8,'tp'=2] {'kv','tp'}, dimensions={0} | all-to-all | bytes 262144 | tf_op jit(solution)/shard_map/all_to_all | solution.py:116
  50.7 2.3 %fusion = bf16[3,16,8,128]{3,2,1,0:T(8,128)(2,1)S(1)} fusion(bf16[512,2048]{1,0:T(8,128)(2,1)S(1)} %copy-done, bf16[2048,512]{1,0:T(8,128)(2,1)} %param.26, f32[24]{0:T(128)S(1)} %add_rsqrt_fusion.2, bf16[16,32,128]{2,1,0:T(8,128)(2,1)S(1)} %all_to_all.26), kind=kOutput, calls=%fused_computation.1 | convolution fusion | flops 100761600 | bytes 4391424 | tf_op jit(solution)/shard_map/dot_general | solution.py:126
  53.0 10.0 %all_to_all.27 = bf16[16,24,128]{2,1,0:T(8,128)(2,1)S(1)} all-to-all(bf16[16,24,128]{2,1,0:T(8,128)(2,1)S(1)} %bitcast.82), channel_id=1, replica_groups=mesh['dp'=2,'kv'=8,'tp'=2] {'kv','tp'}, dimensions={0} | all-to-all | bytes 196608 | tf_op jit(solution)/shard_map/all_to_all | solution.py:127
  63.0 0.6 add_convert_fusion
  (51 shorter events, 1.5 us)
Async XLA Ops:
  0.6 50.0 %copy-start = (bf16[512,2048]{1,0:T(8,128)(2,1)S(1)}, bf16[512,2048]{1,0:T(8,128)(2,1)}, u32[]{:S(2)}) copy-start(bf16[512,2048]{1,0:T(8,128)(2,1)} %param.27) | copy-start | bytes 6291460
  0.6 25.7 %copy-start.1 = (f32[3,4,128,128]{3,2,1,0:T(8,128)S(1)}, f32[3,4,128,128]{3,2,1,0:T(8,128)}, u32[]{:S(2)}) copy-start(f32[3,4,128,128]{3,2,1,0:T(8,128)} %param.15) | copy-start | bytes 2359300
  7.5 25.0 %copy-start.2 = (bf16[512,256]{1,0:T(8,128)(2,1)S(1)}, bf16[512,256]{1,0:T(8,128)(2,1)}, u32[]{:S(2)}) copy-start(bf16[512,256]{1,0:T(8,128)(2,1)} %param.24) | copy-start | bytes 786436
  8.7 24.2 %copy-start.4 = (bf16[128]{0:T(256)(128)(2,1)S(1)}, bf16[128]{0:T(256)(128)(2,1)}, u32[]{:S(2)}) copy-start(bf16[128]{0:T(256)(128)(2,1)} %param.25) | copy-start | bytes 772
  9.9 29.7 %copy-start.3 = (bf16[24,128]{1,0:T(8,128)(2,1)S(1)}, bf16[24,128]{1,0:T(8,128)(2,1)}, u32[]{:S(2)}) copy-start(bf16[24,128]{1,0:T(8,128)(2,1)} %param.14) | copy-start | bytes 18436
  10.6 14.5 %all-to-all-start.1 = ((bf16[8,3,1664]{2,1,0:T(4,128)(2,1)}), bf16[8,3,1664]{2,1,0:T(4,128)(2,1)S(1)}, u32[]{:S(2)}, u32[]{:S(2)}) async-start(bf16[8,3,1664]{2,1,0:T(4,128)(2,1)} %reshape.132), calls=%async_computation.1 | async-start | bytes 212992 | tf_op jit(solution)/shard_map/all_to_all | solution.py:72
  29.0 10.4 %all-to-all-start.2 = ((bf16[16,3,512]{2,1,0:T(4,128)(2,1)}), bf16[16,3,512]{2,1,0:T(4,128)(2,1)S(1)}, u32[]{:S(2)}, u32[]{:S(2)}) async-start(bf16[16,3,512]{2,1,0:T(4,128)(2,1)} %broadcast_in_dim.15), calls=%async_computation.2 | async-start | bytes 131072 | tf_op jit(solution)/shard_map/all_to_all | solution.py:99
  32.6 7.1 %collective-permute-start = (bf16[512,128]{1,0:T(8,128)(2,1)S(1)}, bf16[512,128]{1,0:T(8,128)(2,1)S(1)}, u32[]{:S(2)}, u32[]{:S(2)}) collective-permute-start(bf16[512,128]{1,0:T(8,128)(2,1)S(1)} %constant_dynamic-slice_fusion), channel_id=1, source_target_pairs={{0,1},{1,0},{2,3},{3,2},{4,5},{5,4},{6,7},{7,6},{8,9},{9,8},{10,11... | collective-permute-start | bytes 393224 | tf_op jit(solution)/shard_map/ppermute | solution.py:50
